TPU v7x, 32 devices: a whole 2x2x4 slice. The times are simulated.
32 devices in a mesh: grp: 2 (over x), ep: 16 (over z, y, core).
Axes of the slice: x: 2, y: 2, z: 4, core: 2. Of those that a mesh axis runs over, the one named last changes fastest.
Arguments:
- tokens: bfloat16 [256, 2048], P(('grp', 'ep')), parts along dimension 0, may hold values from -6 to 6
- first_gain: bfloat16 [2048], replicated, may hold values from 0.099609375 to 1.8984375
- query_weight: bfloat16 [2048, 1024], P(None, 'ep'), may hold values from -0.125 to 0.125
- key_weight: bfloat16 [2048, 1024], P(None, 'ep'), may hold values from -0.125 to 0.125
- value_weight: bfloat16 [2048, 1024], P(None, 'ep'), may hold values from -0.125 to 0.125
- outgate_weight: bfloat16 [2048, 1024], P(None, 'ep'), may hold values from -0.125 to 0.125
- igate_weight: bfloat16 [2048, 8], replicated, may hold values from -0.125 to 0.125
- fgate_weight: bfloat16 [2048, 8], replicated, may hold values from -0.125 to 0.125
- igate_bias: float32 [8], replicated, may hold values from -2 to 1
- fgate_bias: float32 [8], replicated, may hold values from -1 to 4
- memory_state: float32 [256, 8, 128, 128], P(('grp', 'ep')), parts along dimension 0, may hold values from -0.6 to 0.6
- norm_state: float32 [256, 8, 128], P(('grp', 'ep')), parts along dimension 0, may hold values from -0.6 to 0.6
- max_state: float32 [256, 8], P(('grp', 'ep')), parts along dimension 0, may hold values from -1 to 2
- head_gain: bfloat16 [1024], replicated, may hold values from 0.099609375 to 1.8984375
- out_weight: bfloat16 [1024, 2048], P('ep'), may hold values from -0.1875 to 0.1875
- second_gain: bfloat16 [2048], replicated, may hold values from 0.099609375 to 1.8984375
- expert_ids: int32 [256, 6], P(('grp', 'ep')), parts along dimension 0, may hold values from 0 to 15, all different within a row; in each aligned block of 8 rows (0 to 7, 8 to 15, ...) at most 6 rows name the same one
- route_weight: float32 [256, 6], P(('grp', 'ep')), parts along dimension 0, may hold values from 0.2 to 1
- expert_gate: bfloat16 [16, 2048, 256], P('ep'), may hold values from -0.125 to 0.125
- expert_up: bfloat16 [16, 2048, 256], P('ep'), may hold values from -0.125 to 0.125
- expert_down: bfloat16 [16, 256, 2048], P('ep'), may hold values from -0.375 to 0.375
- shared_gate: bfloat16 [2048, 256], P('ep'), may hold values from -0.125 to 0.125
- shared_up: bfloat16 [2048, 256], P('ep'), may hold values from -0.125 to 0.125
- shared_down: bfloat16 [256, 2048], P(None, 'ep'), may hold values from -0.375 to 0.375
Outputs:
- mixed_out: bfloat16 [256, 2048], P(('grp', 'ep')), parts along dimension 0
- memory_next: float32 [256, 8, 128, 128], P(('grp', 'ep')), parts along dimension 0
- norm_next: float32 [256, 8, 128], P(('grp', 'ep')), parts along dimension 0
- max_next: float32 [256, 8], P(('grp', 'ep')), parts along dimension 0
There are 2 independent parts, one for each index of `grp`. A program takes and returns all parts, laid end to end along the dimension named above; an argument that names none is the same for every part. Nothing has to cross between parts.
Inputs may be any that keep to these rules, and one draw needn't show every extreme that they name: `expert_ids`: each row names 6 different experts. Among the rows of one device no expert is named by more than 6 rows, and in every draw some expert is named by exactly 6 rows of some device.
All inputs are finite; a program needn't handle non-finite values.
Results may differ from a plain program's by a relative error of at most 0.013.
Values may be sent and summed in bfloat16 or wider, within the bound.
A program may use at most 64 MiB of HBM per device.

v0:
```python
import jax
import jax.numpy as jnp
from jax import lax
from jax.sharding import PartitionSpec as P

epsilon = 1e-06


def rms_scale(values, gain):
    return (
        values
        * lax.rsqrt(jnp.mean(values * values, axis=-1, keepdims=True) + epsilon)
        * gain.astype(jnp.float32)
    )


def cell_step(
    normed,
    query,
    key_proj,
    value_proj,
    outgate,
    igate_weight,
    fgate_weight,
    igate_bias,
    fgate_bias,
    memory_state,
    norm_state,
    max_state,
    head_gain,
):
    row_count, head_count = max_state.shape
    head_size = memory_state.shape[-1]
    input_gate = jnp.dot(normed, igate_weight, preferred_element_type=jnp.float32) + igate_bias
    forget_log = jax.nn.log_sigmoid(
        jnp.dot(normed, fgate_weight, preferred_element_type=jnp.float32) + fgate_bias
    )
    query_heads = query.astype(jnp.float32).reshape(row_count, head_count, head_size)
    key_heads = key_proj.astype(jnp.float32).reshape(
        row_count, head_count, head_size
    ) * head_size ** (-0.5)
    value_heads = value_proj.astype(jnp.float32).reshape(row_count, head_count, head_size)
    max_next = jnp.maximum(forget_log + max_state, input_gate)
    decay_rate = jnp.exp(forget_log + max_state - max_next)
    injected = jnp.exp(input_gate - max_next)
    memory_next = decay_rate[:, :, None, None] * memory_state + injected[:, :, None, None] * (
        key_heads[:, :, :, None] * value_heads[:, :, None, :]
    )
    norm_next = decay_rate[:, :, None] * norm_state + injected[:, :, None] * key_heads
    numerator = jnp.einsum(
        "shd,shde->she", query_heads, memory_next, precision=lax.Precision.HIGHEST
    )
    denominator = jnp.maximum(
        jnp.abs(jnp.sum(query_heads * norm_next, axis=-1)), jnp.exp(-max_next)
    )
    readout = numerator / denominator[:, :, None]
    readout = rms_scale(readout, head_gain.reshape(head_count, head_size))
    gated = readout.reshape(row_count, head_count * head_size) * jax.nn.sigmoid(
        outgate.astype(jnp.float32)
    )
    return (gated.astype(jnp.bfloat16), memory_next, norm_next, max_next)


def shards(
    tokens,
    first_gain,
    query_weight,
    key_weight,
    value_weight,
    outgate_weight,
    igate_weight,
    fgate_weight,
    igate_bias,
    fgate_bias,
    memory_state,
    norm_state,
    max_state,
    head_gain,
    out_weight,
    second_gain,
    expert_ids,
    route_weight,
    expert_gate,
    expert_up,
    expert_down,
    shared_gate,
    shared_up,
    shared_down,
):
    own_rows = tokens.shape[0]
    devices = lax.axis_size("ep")
    top_count = expert_ids.shape[1]
    capacity = max(2, 2 * own_rows * top_count // devices)
    inputs = tokens.astype(jnp.float32)
    normed = rms_scale(inputs, first_gain).astype(jnp.bfloat16)
    block_rows = lax.all_gather(normed, "ep", axis=0, tiled=True)
    columns = jnp.stack(
        [
            jnp.dot(block_rows, matrix, preferred_element_type=jnp.float32).astype(jnp.bfloat16)
            for matrix in (query_weight, key_weight, value_weight, outgate_weight)
        ]
    )
    projected = lax.all_to_all(columns, "ep", split_axis=1, concat_axis=2, tiled=True)
    gated, memory_next, norm_next, max_next = cell_step(
        normed,
        projected[0],
        projected[1],
        projected[2],
        projected[3],
        igate_weight,
        fgate_weight,
        igate_bias,
        fgate_bias,
        memory_state,
        norm_state,
        max_state,
        head_gain,
    )
    picked = gated
    mix_sums = jnp.dot(
        picked,
        lax.all_gather(out_weight, "ep", axis=0, tiled=True),
        preferred_element_type=jnp.float32,
    )
    stream = inputs + mix_sums.astype(jnp.bfloat16).astype(jnp.float32)
    normed_two = rms_scale(stream, second_gain).astype(jnp.bfloat16)
    block_rows = (
        lax.all_gather(shared_gate, "ep", axis=0, tiled=True),
        lax.all_gather(shared_up, "ep", axis=0, tiled=True),
    )
    picked = normed_two
    gate_shared = jnp.dot(picked, block_rows[0], preferred_element_type=jnp.float32)
    up_shared = jnp.dot(picked, block_rows[1], preferred_element_type=jnp.float32)
    hidden_shared = (jax.nn.silu(gate_shared) * up_shared).astype(jnp.bfloat16)
    shared_result = jnp.dot(
        hidden_shared,
        lax.all_gather(shared_down, "ep", axis=1, tiled=True),
        preferred_element_type=jnp.float32,
    )
    choose = (expert_ids[:, :, None] == jnp.arange(devices, dtype=jnp.int32)[None, None, :]).astype(
        jnp.int32
    )
    counted = jnp.sum(choose, axis=1)
    ranking = jnp.cumsum(counted, axis=0) - counted
    slot_index = jnp.sum(choose * ranking[:, None, :], axis=2)
    slot_ids = jnp.arange(capacity, dtype=jnp.int32)
    selector = counted.T[:, None, :] * (ranking.T[:, None, :] == slot_ids[None, :, None]).astype(
        jnp.int32
    )
    outgoing = jnp.einsum(
        "ecr,rd->ecd", selector.astype(jnp.bfloat16), normed_two, preferred_element_type=jnp.float32
    ).astype(jnp.bfloat16)
    arrived = lax.all_to_all(outgoing, "ep", split_axis=0, concat_axis=0, tiled=True)
    sources, slots, width = arrived.shape
    flat_rows = arrived.reshape(sources * slots, width)
    gate_sums = jnp.dot(flat_rows, expert_gate[0], preferred_element_type=jnp.float32)
    up_sums = jnp.dot(flat_rows, expert_up[0], preferred_element_type=jnp.float32)
    hidden = (jax.nn.silu(gate_sums) * up_sums).astype(jnp.bfloat16)
    result = jnp.dot(hidden, expert_down[0], preferred_element_type=jnp.float32).astype(
        jnp.bfloat16
    )
    results = lax.all_to_all(
        result.reshape(sources, slots, width), "ep", split_axis=0, concat_axis=0, tiled=True
    )
    flat_results = results.reshape(devices * capacity, results.shape[2])
    picked_results = flat_results[expert_ids * capacity + slot_index]
    routed = jnp.sum(route_weight[:, :, None] * picked_results.astype(jnp.float32), axis=1)
    mixed_out = (stream + routed + shared_result).astype(jnp.bfloat16)
    return (mixed_out, memory_next, norm_next, max_next)


def solution(mesh):
    placed = (
        P(("grp", "ep"), None),
        P(),
        P(None, "ep"),
        P(None, "ep"),
        P(None, "ep"),
        P(None, "ep"),
        P(),
        P(),
        P(),
        P(),
        P(("grp", "ep"), None, None, None),
        P(("grp", "ep"), None, None),
        P(("grp", "ep"), None),
        P(),
        P("ep", None),
        P(),
        P(("grp", "ep"), None),
        P(("grp", "ep"), None),
        P("ep", None, None),
        P("ep", None, None),
        P("ep", None, None),
        P("ep", None),
        P("ep", None),
        P(None, "ep"),
    )
    return jax.shard_map(
        shards,
        mesh=mesh,
        in_specs=placed,
        out_specs=(
            P(("grp", "ep"), None),
            P(("grp", "ep"), None, None, None),
            P(("grp", "ep"), None, None),
            P(("grp", "ep"), None),
        ),
        check_vma=False,
    )
```

profile of v0, /device:TPU:0, one launch (start us, length us, event | category | flops | bytes accessed | tf_op | source)
XLA Modules:
  0.0 194.8 jit_solution(18335394254270634756)
XLA Ops:
  7.2 0.0 copy-start
  7.3 0.0 all-gather.5.cloned.1.call-start
  7.3 0.7 all-gather.5.cloned.1.call-update
  8.0 0.0 all-gather.7.cloned.1.call-start
  8.1 0.7 all-gather.7.cloned.1.call-update
  8.8 0.7 convert_element_type.101
  9.4 0.9 fusion.20
  10.3 0.8 fusion.22
  11.2 25.4 %all_gather.15 = bf16[128,2048]{1,0:T(8,128)(2,1)S(1)} all-gather(bf16[8,2048]{1,0:T(8,128)(2,1)S(1)} %fusion.22), channel_id=1, replica_groups=mesh['grp'=2,'ep'=16] {'ep'}, dimensions={0}, use_global_device_ids=true | all-gather | bytes 557056 | tf_op jit(solution)/shard_map/all_gather | solution.py:96
  36.6 1.2 fusion.4
  37.9 1.3 fusion.5
  39.1 1.2 fusion.6
  40.4 1.3 fusion.7
  41.7 0.1 copy.50
  41.8 0.8 reshape.131
  42.6 3.5 %all-to-all-start = ((bf16[16,2,1024]{2,1,0:T(2,128)(2,1)}), bf16[16,2,1024]{2,1,0:T(2,128)(2,1)S(1)}, u32[]{:S(2)}, u32[]{:S(2)}) async-start(bf16[16,2,1024]{2,1,0:T(2,128)(2,1)} %reshape.131), calls=%async_computation | async-start | bytes 131072 | tf_op jit(solution)/shard_map/all_to_all | solution.py:103
  46.1 0.0 all-gather.11.cloned.1.call-start
  46.1 0.7 all-gather.11.cloned.1.call-update
  46.9 0.1 convolution_add_fusion.1
  47.0 0.1 subtract_exponential_fusion.1
  47.2 0.1 copy.57
  47.3 0.1 convert_reduce_fusion
  47.4 7.0 %all-to-all-done = bf16[16,2,1024]{2,1,0:T(2,128)(2,1)S(1)} async-done(((bf16[16,2,1024]{2,1,0:T(2,128)(2,1)}), bf16[16,2,1024]{2,1,0:T(2,128)(2,1)S(1)}, u32[]{:S(2)}, u32[]{:S(2)}) %all-to-all-start) | async-done | bytes 65568 | tf_op jit(solution)/shard_map/all_to_all | solution.py:103
  54.4 0.1 reshape.132
  54.6 0.1 reshape.105
  54.7 0.1 reshape.130
  54.8 0.1 reshape.110
  54.9 0.1 reshape.111
  55.0 0.7 multiply_reduce_fusion.3
  55.7 0.1 copy.55
  55.8 0.1 reshape.114
  55.9 3.7 %multiply_add_fusion = f32[8,8,128,128]{3,2,1,0:T(8,128)S(1)} fusion(f32[8,8,128,128]{3,2,1,0:T(8,128)} %param.34, f32[8,8,128]{2,1,0:T(8,128)S(1)} %reshape.111, f32[8,8,128]{2,1,0:T(8,128)S(1)} %get-tuple-element.13, f32[8,8]{1,0:T(8,128)S(1)} %get-tuple-element.9, f32[8,8]{1,0:T(8,128)S(1)} %get-tuple-element.6), kind=kLoop, calls=%fused_computation.1 | loop fusion | flops 4194304 | bytes 8454656 | tf_op jit(solution)/shard_map/add | solution.py:46
  59.6 0.0 copy-start.1
  59.7 2.0 %copy-done.1 = f32[8,8,128,128]{3,2,1,0:T(8,128)} copy-done((f32[8,8,128,128]{3,2,1,0:T(8,128)}, f32[8,8,128,128]{3,2,1,0:T(8,128)S(1)}, u32[]{:S(2)}) %copy-start.1) | copy-done | bytes 4194328
  61.7 2.0 %fusion.44 = f32[8,8,1,128]{3,2,1,0:T(1,128)S(1)} fusion(bf16[8,8,128,1]{2,3,1,0:T(2,128)(2,1)S(1)} %reshape.130, f32[8,8,128,128]{3,2,1,0:T(8,128)S(1)} %multiply_add_fusion), kind=kOutput, calls=%fused_computation.89 | convolution fusion | flops 12582912 | bytes 4243456 | tf_op jit(solution)/shard_map/shd,shde->she/dot_general | solution.py:50
  63.7 0.2 multiply_reduce_fusion.2
  63.8 0.0 copy-start.2
  63.9 1.1 all-gather.5.cloned.1.call-done
  64.9 3.0 %multiply_reduce_fusion.1 = (f32[8]{0:T(128)S(1)}, f32[8,2048]{1,0:T(8,128)S(1)}) fusion(bf16[1024,2048]{1,0:T(8,128)(2,1)} %all-gather.5.cloned.1.call-done, f32[8,1024]{1,0:T(8,128)S(1)} %reshape.114, f32[8,128]{1,0:T(8,128)S(1)} %bitcast_convert_fusion, f32[8,8]{0,1:T(8,128)S(1)} %add_rsqrt_fusion, f32[8,8]{0,1:T(8,128)S(1)} %copy.55, ...), kind=kOutput, calls=%fused_computation.42 | convolution fusion | flops 33693688 | bytes 4362784 | tf_op jit(solution)/shard_map/dot_general | solution.py:120
  67.9 0.3 convolution_convert_fusion.1
  68.3 1.1 copy.58
  69.3 3.6 %all-to-all-start.1 = ((bf16[16,6,2048]{2,1,0:T(8,128)(2,1)}), bf16[16,6,2048]{2,1,0:T(8,128)(2,1)S(1)}, u32[]{:S(2)}, u32[]{:S(2)}) async-start(bf16[16,6,2048]{2,1,0:T(8,128)(2,1)} %copy.58), calls=%async_computation.1 | async-start | bytes 1048576 | tf_op jit(solution)/shard_map/all_to_all | solution.py:153
  72.9 0.0 all-gather.9.cloned.1.call-start
  73.0 0.5 all-gather.9.cloned.1.call-update
  73.5 15.8 %all-to-all-done.1 = bf16[16,6,2048]{2,1,0:T(8,128)(2,1)S(1)} async-done(((bf16[16,6,2048]{2,1,0:T(8,128)(2,1)}), bf16[16,6,2048]{2,1,0:T(8,128)(2,1)S(1)}, u32[]{:S(2)}, u32[]{:S(2)}) %all-to-all-start.1) | async-done | bytes 393248 | tf_op jit(solution)/shard_map/all_to_all | solution.py:153
  89.3 0.1 reshape.107
  89.4 1.5 fusion.13
  91.0 0.8 convolution_convert_fusion
  91.8 0.0 copy-start.8
  91.8 1.0 reshape.108
  92.7 4.2 %all-to-all-start.2 = ((bf16[16,6,2048]{2,1,0:T(8,128)(2,1)}), bf16[16,6,2048]{2,1,0:T(8,128)(2,1)S(1)}, u32[]{:S(2)}, u32[]{:S(2)}) async-start(bf16[16,6,2048]{2,1,0:T(8,128)(2,1)} %reshape.108), calls=%async_computation.2 | async-start | bytes 1048576 | tf_op jit(solution)/shard_map/all_to_all | solution.py:162
  97.0 0.2 select_reduce_fusion
  97.3 0.1 copy.60
  97.4 0.1 reshape.117
  97.4 10.2 %all-gather.7.cloned.1.call-done = bf16[2048,256]{1,0:T(8,128)(2,1)} async-done(((bf16[128,256]{1,0:T(8,128)(2,1)}), bf16[2048,256]{1,0:T(8,128)(2,1)}) %all-gather.7.cloned.1.call-update) | async-done | bytes 1048592 | tf_op jit(solution)/shard_map/all_gather | solution.py:128
  107.7 1.5 fusion.43
  109.2 2.7 %all-to-all-done.2 = bf16[16,6,2048]{2,1,0:T(8,128)(2,1)S(1)} async-done(((bf16[16,6,2048]{2,1,0:T(8,128)(2,1)}), bf16[16,6,2048]{2,1,0:T(8,128)(2,1)S(1)}, u32[]{:S(2)}, u32[]{:S(2)}) %all-to-all-start.2) | async-done | bytes 393248 | tf_op jit(solution)/shard_map/all_to_all | solution.py:162
  111.8 0.1 reshape.109
  112.0 0.7 gather_fusion
  112.7 0.1 reshape.125
  112.8 0.2 multiply_reduce_fusion
  113.0 32.8 %all-gather.11.cloned.1.call-done = bf16[256,2048]{1,0:T(8,128)(2,1)} async-done(((bf16[256,128]{1,0:T(8,128)(2,1)}), bf16[256,2048]{1,0:T(8,128)(2,1)}) %all-gather.11.cloned.1.call-update) | async-done | bytes 1048592 | tf_op jit(solution)/shard_map/all_gather | solution.py:137
  145.8 39.5 %all-gather.9.cloned.1.call-done = bf16[2048,256]{1,0:T(8,128)(2,1)} async-done(((bf16[128,256]{1,0:T(8,128)(2,1)}), bf16[2048,256]{1,0:T(8,128)(2,1)}) %all-gather.9.cloned.1.call-update) | async-done | bytes 1048592 | tf_op jit(solution)/shard_map/all_gather | solution.py:129
  185.3 2.9 %fusion = bf16[8,2048]{1,0:T(8,128)(2,1)} fusion(bf16[256,2048]{1,0:T(8,128)(2,1)} %all-gather.11.cloned.1.call-done, bf16[2048,256]{1,0:T(8,128)(2,1)} %all-gather.9.cloned.1.call-done, f32[8,2048]{1,0:T(8,128)S(1)} %get-tuple-element.15, f32[8,2048]{1,0:T(8,128)S(1)} %multiply_reduce_fusion, f32[8,256]{1,0:T(8,128)S(1)} %fusion.43, ...), kind=kOutput, calls=%fused_computation.5 | convolution fusion | flops 16887808 | bytes 2277408 | tf_op jit(solution)/shard_map/dot_general | solution.py:135
  (45 shorter events, 0.3 us)
Async XLA Ops:
  7.2 83.8 %copy-start = (bf16[1,256,2048]{2,1,0:T(8,128)(2,1)S(1)}, bf16[1,256,2048]{2,1,0:T(8,128)(2,1)}, u32[]{:S(2)}) copy-start(bf16[1,256,2048]{2,1,0:T(8,128)(2,1)} %param.44) | copy-start | bytes 3145732
  7.2 39.6 %copy-start.6 = (bf16[2048,8]{0,1:T(8,128)(2,1)S(1)}, bf16[2048,8]{0,1:T(8,128)(2,1)}, u32[]{:S(2)}) copy-start(bf16[2048,8]{0,1:T(8,128)(2,1)} %param.30) | copy-start | bytes 98308
  7.2 39.6 %copy-start.13 = (f32[8]{0:T(128)S(1)}, f32[8]{0:T(128)}, u32[]{:S(2)}) copy-start(f32[8]{0:T(128)} %param.32) | copy-start | bytes 100
  7.2 39.8 %copy-start.7 = (bf16[2048,8]{0,1:T(8,128)(2,1)S(1)}, bf16[2048,8]{0,1:T(8,128)(2,1)}, u32[]{:S(2)}) copy-start(bf16[2048,8]{0,1:T(8,128)(2,1)} %param.31) | copy-start | bytes 98308
  7.2 39.8 %copy-start.14 = (f32[8]{0:T(128)S(1)}, f32[8]{0:T(128)}, u32[]{:S(2)}) copy-start(f32[8]{0:T(128)} %param.33) | copy-start | bytes 100
  7.2 39.8 %copy-start.9 = (f32[8,8]{1,0:T(8,128)S(1)}, f32[8,8]{1,0:T(8,128)}, u32[]{:S(2)}) copy-start(f32[8,8]{1,0:T(8,128)} %param.36) | copy-start | bytes 772
  7.2 39.9 %copy-start.10 = (bf16[2048]{0:T(1024)(128)(2,1)S(1)}, bf16[2048]{0:T(1024)(128)(2,1)}, u32[]{:S(2)}) copy-start(bf16[2048]{0:T(1024)(128)(2,1)} %param.39) | copy-start | bytes 12292
  7.2 40.0 %copy-start.11 = (s32[8,6]{1,0:T(8,128)S(1)}, s32[8,6]{1,0:T(8,128)}, u32[]{:S(2)}) copy-start(s32[8,6]{1,0:T(8,128)} %param.40) | copy-start | bytes 580
  7.3 40.2 %copy-start.12 = (bf16[1024]{0:T(1024)(128)(2,1)S(1)}, bf16[1024]{0:T(1024)(128)(2,1)}, u32[]{:S(2)}) copy-start(bf16[1024]{0:T(1024)(128)(2,1)} %param.37) | copy-start | bytes 6148
  7.3 47.8 %copy-start.5 = (f32[8,8,128]{2,1,0:T(8,128)S(1)}, f32[8,8,128]{2,1,0:T(8,128)}, u32[]{:S(2)}) copy-start(f32[8,8,128]{2,1,0:T(8,128)} %param.35) | copy-start | bytes 98308
  7.3 57.6 %all-gather.5.cloned.1.call-start = ((), (), s32[]{:S(2)}) async-start(), calls=%async_computation.3 | async-start | bytes 4456448 | tf_op jit(solution)/shard_map/all_gather | solution.py:122
  8.0 99.7 %all-gather.7.cloned.1.call-start = ((), (), s32[]{:S(2)}) async-start(), calls=%async_computation.4 | async-start | bytes 1114112 | tf_op jit(solution)/shard_map/all_gather | solution.py:128
  42.6 11.8 %all-to-all-start = ((bf16[16,2,1024]{2,1,0:T(2,128)(2,1)}), bf16[16,2,1024]{2,1,0:T(2,128)(2,1)S(1)}, u32[]{:S(2)}, u32[]{:S(2)}) async-start(bf16[16,2,1024]{2,1,0:T(2,128)(2,1)} %reshape.131), calls=%async_computation | async-start | bytes 131072 | tf_op jit(solution)/shard_map/all_to_all | solution.py:103
  46.1 99.7 %all-gather.11.cloned.1.call-start = ((), (), s32[]{:S(2)}) async-start(), calls=%async_computation.6 | async-start | bytes 1114112 | tf_op jit(solution)/shard_map/all_gather | solution.py:137
  47.2 12.5 %copy-start.4 = (f32[8,8]{1,0:T(8,128)}, f32[8,8]{1,0:T(8,128)S(1)}, u32[]{:S(2)}) copy-start(f32[8,8]{1,0:T(8,128)S(1)} %get-tuple-element.7) | copy-start | bytes 772
  59.6 2.0 %copy-start.1 = (f32[8,8,128,128]{3,2,1,0:T(8,128)}, f32[8,8,128,128]{3,2,1,0:T(8,128)S(1)}, u32[]{:S(2)}) copy-start(f32[8,8,128,128]{3,2,1,0:T(8,128)S(1)} %multiply_add_fusion) | copy-start | bytes 12582916
  61.7 3.3 %copy-start.3 = (bf16[8,2048]{1,0:T(8,128)(2,1)S(1)}, bf16[8,2048]{1,0:T(8,128)(2,1)}, u32[]{:S(2)}) copy-start(bf16[8,2048]{1,0:T(8,128)(2,1)} %param.24) | copy-start | bytes 98308
  63.8 27.1 %copy-start.2 = (bf16[1,2048,256]{2,1,0:T(8,128)(2,1)S(1)}, bf16[1,2048,256]{2,1,0:T(8,128)(2,1)}, u32[]{:S(2)}) copy-start(bf16[1,2048,256]{2,1,0:T(8,128)(2,1)} %param.43) | copy-start | bytes 3145732
  69.3 20.0 %all-to-all-start.1 = ((bf16[16,6,2048]{2,1,0:T(8,128)(2,1)}), bf16[16,6,2048]{2,1,0:T(8,128)(2,1)S(1)}, u32[]{:S(2)}, u32[]{:S(2)}) async-start(bf16[16,6,2048]{2,1,0:T(8,128)(2,1)} %copy.58), calls=%async_computation.1 | async-start | bytes 1048576 | tf_op jit(solution)/shard_map/all_to_all | solution.py:153
  72.9 112.4 %all-gather.9.cloned.1.call-start = ((), (), s32[]{:S(2)}) async-start(), calls=%async_computation.5 | async-start | bytes 1114112 | tf_op jit(solution)/shard_map/all_gather | solution.py:129
  91.8 21.0 %copy-start.8 = (f32[8,6]{1,0:T(8,128)S(1)}, f32[8,6]{1,0:T(8,128)}, u32[]{:S(2)}) copy-start(f32[8,6]{1,0:T(8,128)} %param.41) | copy-start | bytes 580
  92.7 19.1 %all-to-all-start.2 = ((bf16[16,6,2048]{2,1,0:T(8,128)(2,1)}), bf16[16,6,2048]{2,1,0:T(8,128)(2,1)S(1)}, u32[]{:S(2)}, u32[]{:S(2)}) async-start(bf16[16,6,2048]{2,1,0:T(8,128)(2,1)} %reshape.108), calls=%async_computation.2 | async-start | bytes 1048576 | tf_op jit(solution)/shard_map/all_to_all | solution.py:162
Sparse Core Ops, SparseCore 0:
  10.2 54.6 all-gather.4
  67.1 40.5 all-gather.6
  109.8 35.8 all-gather.10
  147.8 37.4 all-gather.8
where the time goes:
time: 196 us; the launch traced here: 195 us
  waiting for transfers between devices  112 us (57%)
  blocking collectives  25.4 us (13%)
  matrix products  17.4 us (9%)
  between operations  14.2 us (7%)
  starting transfers between devices  11.5 us (6%)
  other arithmetic  7.7 us (4%)
  local copies, waits for them, and re-layouts  6.97 us (4%)
    all_gather x1, waiting for transfers between devices, shards(): lax.all_gather(shared_up, 'ep', axis=0, tiled=True)  39.5 us
    all_gather x1, waiting for transfers between devices, shards(): lax.all_gather(shared_down, 'ep', axis=1, tiled=True)  32.8 us
    all_gather x1, blocking collectives, shards(): block_rows = lax.all_gather(normed, 'ep', axis=0, tiled=True)  25.4 us
    all_to_all x1, waiting for transfers between devices, shards(): lax.all_to_all(outgoing, 'ep', split_axis=0, concat_axis=0, tiled=True)  15.8 us
    all_gather x1, waiting for transfers between devices, shards(): lax.all_gather(shared_gate, 'ep', axis=0, tiled=True)  10.2 us
    all_to_all x1, waiting for transfers between devices, shards(): lax.all_to_all(columns, 'ep', split_axis=1, concat_axis=2, tiled=True)  6.97 us
    dot_general x4, matrix products, shards(): jnp.dot(block_rows, matrix, preferred_element_type=jnp.float32)  5.03 us
    all_to_all x1, starting transfers between devices, shards(): lax.all_to_all(result.reshape(sources, slots, width), 'ep', split_axis=0,...  4.24 us
  transfers between devices with their start and end apart: 7, of which 7 were waited for; matrix products, arithmetic and copies ran while one was open for 14% of the time, Pallas kernels for 0%

commit v1 on v0

--- a/solution.py
+++ b/solution.py
@@ -1,7 +1,10 @@
 import jax
 import jax.numpy as jnp
 from jax import lax
+from jax.experimental import pallas as pl
+from jax.experimental.pallas import tpu as pltpu
 from jax.sharding import PartitionSpec as P
+import functools
 
 epsilon = 1e-06
 
@@ -169,6 +172,453 @@
     return (mixed_out, memory_next, norm_next, max_next)
 
 
+ANY, VMEM = pl.ANY, pltpu.VMEM
+F32, BF16 = jnp.float32, jnp.bfloat16
+
+
+def remote(source, target, send, receive, device):
+    return pltpu.make_async_remote_copy(
+        src_ref=source,
+        dst_ref=target,
+        send_sem=send,
+        recv_sem=receive,
+        device_id={"ep": device},
+        device_id_type=pl.DeviceIdType.MESH,
+    )
+
+
+def fused(
+    n,
+    tokens,
+    first_gain,
+    query_weight,
+    key_weight,
+    value_weight,
+    outgate_weight,
+    igate_weight,
+    fgate_weight,
+    igate_bias,
+    fgate_bias,
+    memory_state,
+    norm_state,
+    max_state,
+    head_gain,
+    out_weight,
+    second_gain,
+    expert_ids,
+    route_weight,
+    expert_gate,
+    expert_up,
+    expert_down,
+    shared_gate,
+    shared_up,
+    shared_down,
+    mixed_out,
+    memory_next,
+    norm_next,
+    max_next,
+    proj_in,
+    proj,
+    gates_in,
+    memory,
+    out_pad,
+    wide,
+    down,
+    rows_one,
+    rows_two,
+    table,
+    column_send,
+    column_recv,
+    shared_send,
+    shared_recv,
+    sdown_recv,
+    gated_send,
+    gated_recv,
+    part,
+    part_send,
+    pair_recv,
+    sum_send,
+    sum_recv,
+    local_sem,
+    memory_in_sem,
+    memory_out_sem,
+    send_sem,
+    recv_sem,
+    gather_sem,
+    pair_sem,
+    sum_sem,
+):
+    rows, width = tokens.shape
+    heads, size = memory_state.shape[1], memory_state.shape[3]
+    cut = query_weight.shape[1]
+    share = size // cut
+    hidden = shared_gate.shape[1] // n
+    top_count = expert_ids.shape[1]
+    chips = n // 2
+    me = lax.axis_index("ep")
+    side, chip = me % 2, me // 2
+    partner = me + 1 - 2 * side
+
+    barrier = pltpu.get_barrier_semaphore()
+    for k in range(1, n):
+        pl.semaphore_signal(
+            barrier,
+            inc=1,
+            device_id={"ep": (me + k) % n},
+            device_id_type=pl.DeviceIdType.MESH,
+        )
+
+    loads = []
+
+    def load(source, target):
+        copy = pltpu.make_async_copy(source, target, local_sem.at[len(loads)])
+        copy.start()
+        loads.append(copy)
+        return copy
+
+    proj_loads = [
+        load(matrix, proj_in.at[i])
+        for i, matrix in enumerate((query_weight, key_weight, value_weight, outgate_weight))
+    ]
+    gate_loads = [load(igate_weight, gates_in.at[0]), load(fgate_weight, gates_in.at[1])]
+    memory_loads = []
+    for h in range(heads):
+        copy = pltpu.make_async_copy(
+            memory_state.at[:, h], memory.at[:, h], memory_in_sem.at[h]
+        )
+        copy.start()
+        memory_loads.append(copy)
+    spot = pl.multiple_of((me % share) * cut, cut)
+    out_load = load(out_weight, out_pad.at[pl.ds(spot, cut)])
+    wide_loads = [load(expert_gate.at[0], wide.at[0]), load(expert_up.at[0], wide.at[1])]
+    down_load = load(expert_down.at[0], down)
+
+    inputs = tokens[...].astype(F32)
+    rows_one[me] = rms_scale(inputs, first_gain[...]).astype(BF16)
+
+    pl.semaphore_wait(barrier, n - 1)
+
+    def gather(buffer, which):
+        sends = []
+        for k in range(chips - 1, 0, -1):
+            there = 2 * ((chip + k) % chips) + side
+            sends.append(
+                remote(
+                    buffer.at[me],
+                    buffer.at[me],
+                    gather_sem.at[which, 0, k],
+                    gather_sem.at[which, 1, k],
+                    there,
+                )
+            )
+            sends[-1].start()
+        near = remote(
+            buffer.at[me],
+            buffer.at[me],
+            gather_sem.at[which, 2, 0],
+            gather_sem.at[which, 3, 0],
+            partner,
+        )
+        near.start()
+        return sends, near
+
+    def gather_end(buffer, which, sends, near):
+        passed = [near]
+        for k in ORDER(chips):
+            slot = 2 * ((chip + chips - k) % chips) + side
+            sends[chips - 1 - k].wait_recv()
+            onward = remote(
+                buffer.at[slot],
+                buffer.at[slot],
+                gather_sem.at[which, 2, k],
+                gather_sem.at[which, 3, k],
+                partner,
+            )
+            onward.start()
+            passed.append(onward)
+        for copy in passed:
+            copy.wait_recv()
+        return sends + passed
+
+    unsent = []
+    first = gather(rows_one, 0)
+
+    for copy in proj_loads:
+        copy.wait()
+    for i in range(4):
+        proj[:, i * cut : (i + 1) * cut] = proj_in[i]
+    for i in range(1, share):
+        other = pl.multiple_of(((me + i) % share) * cut, cut)
+        out_pad[pl.ds(other, cut), :] = jnp.zeros((cut, width), BF16)
+    lanes = lax.broadcasted_iota(jnp.int32, (rows, 128), 1)
+    routes = jnp.zeros((rows, 128), F32)
+    for t in range(top_count):
+        routes = routes + jnp.where(
+            expert_ids[:, t : t + 1] == lanes, route_weight[:, t : t + 1], 0.0
+        )
+    table[me] = routes
+    for i, matrix in enumerate((shared_gate, shared_up)):
+        turned = matrix[...].astype(F32).T.reshape(n, hidden, matrix.shape[0])
+        shared_send[:, i * hidden : (i + 1) * hidden, :] = turned.astype(BF16)
+    for copy in gate_loads:
+        copy.wait()
+    own = rows_one[me]
+    input_gate = jnp.dot(own, gates_in[0], preferred_element_type=F32) + igate_bias[...]
+    forget_log = jax.nn.log_sigmoid(
+        jnp.dot(own, gates_in[1], preferred_element_type=F32) + fgate_bias[...]
+    )
+    kept = forget_log + max_state[...]
+    top = jnp.maximum(kept, input_gate)
+    max_next[...] = top
+    decay_rate = jnp.exp(kept - top)
+    injected = jnp.exp(input_gate - top)
+    floor = jnp.exp(-top)
+
+    unsent += gather_end(rows_one, 0, *first)
+
+    def flat(buffer):
+        held = buffer[...].astype(F32)
+        return held.reshape(n * rows, held.shape[2])
+
+    columns = jnp.dot(flat(rows_one).astype(BF16), proj[...], preferred_element_type=F32)
+    column_send[...] = columns.reshape(n, rows, 4 * cut).astype(BF16)
+
+    def spread(which, source, target):
+        for k in range(1, n):
+            there = (me + k) % n
+            copy = remote(
+                source(there), target, send_sem.at[which, k], recv_sem.at[which, k], there
+            )
+            copy.start()
+            unsent.append(copy)
+
+    def arrive(which, source, target):
+        for k in range(1, n):
+            remote(
+                source(me), target, send_sem.at[which, k], recv_sem.at[which, k], (me + k) % n
+            ).wait_recv()
+
+    spread(0, lambda j: column_send.at[j], column_recv.at[me])
+    column_recv[me] = column_send[me]
+    spread(1, lambda j: table.at[me], table.at[me])
+    arrive(0, lambda j: column_send.at[j], column_recv.at[me])
+    spread(2, lambda j: shared_send.at[j], shared_recv.at[me])
+    shared_recv[me] = shared_send[me]
+    spread(3, lambda j: shared_down.at[j], sdown_recv.at[me])
+    sdown_recv[me] = shared_down[me]
+
+    memory_stores = []
+    for h in range(heads):
+        pieces = [column_recv[h * share + i].astype(F32) for i in range(share)]
+        query, keyed, valued, outgate = [
+            jnp.concatenate([piece[:, i * cut : (i + 1) * cut] for piece in pieces], axis=1)
+            for i in range(4)
+        ]
+        decay = jnp.broadcast_to(decay_rate[:, h : h + 1], (rows, size))
+        inject = keyed * size ** (-0.5) * injected[:, h : h + 1]
+        norm = decay * norm_state[:, h, :] + inject
+        norm_next[:, h, :] = norm
+        bottom = jnp.maximum(
+            jnp.abs(jnp.sum(query * norm, axis=-1, keepdims=True)), floor[:, h : h + 1]
+        )
+        key_columns, query_columns = inject.T, query.T
+        memory_loads[h].wait()
+        tops = []
+        for s in range(rows):
+            cell = (
+                decay[s : s + 1, :] * memory[s, h]
+                + key_columns[:, s : s + 1] * valued[s : s + 1, :]
+            )
+            memory[s, h] = cell
+            tops.append(jnp.sum(query_columns[:, s : s + 1] * cell, axis=0, keepdims=True))
+        store = pltpu.make_async_copy(
+            memory.at[:, h], memory_next.at[:, h], memory_out_sem.at[h]
+        )
+        store.start()
+        memory_stores.append(store)
+        readout = jnp.concatenate(tops, axis=0) / bottom
+        readout = rms_scale(readout, head_gain[h : h + 1, :])
+        gated_send[h] = (readout * jax.nn.sigmoid(outgate)).astype(BF16)
+
+    spread(4, lambda j: gated_send.at[j // share], gated_recv.at[me])
+    gated_recv[me] = gated_send[me // share]
+    out_load.wait()
+    arrive(4, lambda j: gated_send.at[j // share], gated_recv.at[me])
+
+    def scatter(which, total, value):
+        part[...] = value.reshape(n, rows, width)
+        pair = []
+        for k in list(range(1, chips)) + [0]:
+            c = (chip + k) % chips
+            part_send[which, c] = part[2 * c + 1 - side].astype(BF16)
+            copy = remote(
+                part_send.at[which, c],
+                pair_recv.at[which, c],
+                pair_sem.at[which, 0, k],
+                pair_sem.at[which, 1, k],
+                partner,
+            )
+            copy.start()
+            pair.append((k, c, copy))
+        sends = []
+        for k, c, copy in pair:
+            copy.wait_recv()
+            both = part[2 * c + side] + pair_recv[which, c].astype(F32)
+            if k == 0:
+                total = total + both if total is not None else both
+                continue
+            sum_send[which, c] = both.astype(BF16)
+            away = remote(
+                sum_send.at[which, c],
+                sum_recv.at[which, chip],
+                sum_sem.at[which, 0, k],
+                sum_sem.at[which, 1, k],
+                2 * c + side,
+            )
+            away.start()
+            sends.append((k, away))
+        for k, away in sends:
+            away.wait_recv()
+            total = total + sum_recv[which, (chip + chips - k) % chips].astype(F32)
+        unsent.extend([copy for _, _, copy in pair] + [away for _, away in sends])
+        return total
+
+    mix = scatter(
+        0, None, jnp.dot(flat(gated_recv).astype(BF16), out_pad[...], preferred_element_type=F32)
+    )
+    stream = tokens[...].astype(F32) + mix.astype(BF16).astype(F32)
+    rows_two[me] = rms_scale(stream, second_gain[...]).astype(BF16)
+    second = gather(rows_two, 1)
+    for copy in wide_loads + [down_load]:
+        copy.wait()
+    arrive(1, lambda j: table.at[me], table.at[me])
+    arrive(2, lambda j: shared_send.at[j], shared_recv.at[me])
+    arrive(3, lambda j: shared_down.at[j], sdown_recv.at[me])
+    weights = flat(table)
+    mine = lax.broadcasted_iota(jnp.int32, weights.shape, 1) == me
+    weight = jnp.sum(jnp.where(mine, weights, 0.0), axis=1, keepdims=True)
+    shared_wide = jnp.concatenate([shared_recv[i] for i in range(n)], axis=1)
+    shared_rows = jnp.concatenate([sdown_recv[i] for i in range(n)], axis=1)
+    unsent += gather_end(rows_two, 1, *second)
+
+    block = flat(rows_two).astype(BF16)
+    gate_sums = jnp.dot(block, wide[0], preferred_element_type=F32)
+    up_sums = jnp.dot(block, wide[1], preferred_element_type=F32)
+    own_hidden = (jax.nn.silu(gate_sums) * up_sums).astype(BF16)
+    both = lax.dot_general(
+        block, shared_wide, (((1,), (1,)), ((), ())), preferred_element_type=F32
+    )
+    shared_hidden = (jax.nn.silu(both[:, :hidden]) * both[:, hidden:]).astype(BF16)
+    value = weight * jnp.dot(own_hidden, down[...], preferred_element_type=F32) + jnp.dot(
+        shared_hidden, shared_rows, preferred_element_type=F32
+    )
+    mixed_out[...] = scatter(1, stream, value).astype(BF16)
+
+    for copy in unsent:
+        copy.wait_send()
+    for copy in memory_stores:
+        copy.wait()
+
+
+def ORDER(chips):
+    return range(chips - 1, 0, -1)
+
+
+def fused_shards(n, *args):
+    (tokens, first_gain, query_weight, key_weight, value_weight, outgate_weight, igate_weight,
+     fgate_weight, igate_bias, fgate_bias, memory_state, norm_state, max_state, head_gain,
+     out_weight, second_gain, expert_ids, route_weight, expert_gate, expert_up, expert_down,
+     shared_gate, shared_up, shared_down) = args
+    rows, width = tokens.shape
+    heads, size = memory_state.shape[1], memory_state.shape[3]
+    cut = query_weight.shape[1]
+    hidden = shared_gate.shape[1] // n
+    chips = n // 2
+    inner = expert_gate.shape[2]
+    operands = (
+        tokens, first_gain.reshape(1, -1), query_weight, key_weight, value_weight, outgate_weight,
+        igate_weight, fgate_weight, igate_bias.reshape(1, -1), fgate_bias.reshape(1, -1),
+        memory_state, norm_state, max_state, head_gain.reshape(heads, size), out_weight,
+        second_gain.reshape(1, -1), expert_ids, route_weight, expert_gate, expert_up, expert_down,
+        shared_gate, shared_up, shared_down.reshape(n, hidden, shared_down.shape[1]),
+    )
+    far = {2, 3, 4, 5, 6, 7, 10, 14, 18, 19, 20}
+    dma = pltpu.SemaphoreType.DMA
+    return pl.pallas_call(
+        functools.partial(fused, n),
+        out_shape=(
+            jax.ShapeDtypeStruct((rows, width), BF16),
+            jax.ShapeDtypeStruct(memory_state.shape, F32),
+            jax.ShapeDtypeStruct(norm_state.shape, F32),
+            jax.ShapeDtypeStruct(max_state.shape, F32),
+        ),
+        in_specs=[
+            pl.BlockSpec(memory_space=ANY if i in far else VMEM) for i in range(len(operands))
+        ],
+        out_specs=tuple(pl.BlockSpec(memory_space=m) for m in (VMEM, ANY, VMEM, VMEM)),
+        scratch_shapes=[
+            VMEM((4, width, cut), BF16),
+            VMEM((width, 4 * cut), BF16),
+            VMEM((2, width, heads), BF16),
+            VMEM(memory_state.shape, F32),
+            VMEM((size, width), BF16),
+            VMEM((2, width, inner), BF16),
+            VMEM((inner, width), BF16),
+            VMEM((n, rows, width), BF16),
+            VMEM((n, rows, width), BF16),
+            VMEM((n, rows, 128), F32),
+            VMEM((n, rows, 4 * cut), BF16),
+            VMEM((n, rows, 4 * cut), BF16),
+            VMEM((n, 2 * hidden, shared_gate.shape[0]), BF16),
+            VMEM((n, 2 * hidden, shared_gate.shape[0]), BF16),
+            VMEM((n, hidden, shared_down.shape[1]), BF16),
+            VMEM((heads, rows, size), BF16),
+            VMEM((n, rows, size), BF16),
+            VMEM((n, rows, width), F32),
+            VMEM((2, chips, rows, width), BF16),
+            VMEM((2, chips, rows, width), BF16),
+            VMEM((2, chips, rows, width), BF16),
+            VMEM((2, chips, rows, width), BF16),
+            dma((10,)),
+            dma((heads,)),
+            dma((heads,)),
+            dma((5, n)),
+            dma((5, n)),
+            dma((2, 4, chips)),
+            dma((2, 2, chips)),
+            dma((2, 2, chips)),
+        ],
+        compiler_params=pltpu.CompilerParams(
+            collective_id=0, has_side_effects=True, vmem_limit_bytes=60 * 1024 * 1024
+        ),
+    )(*operands)
+
+
+def fits(n, width, size, cut, hidden_all, experts, rows):
+    return (
+        n % 2 == 0
+        and n <= 128
+        and experts == n
+        and width % (128 * n) == 0
+        and hidden_all % (16 * n) == 0
+        and size == 128
+        and size % cut == 0
+        and cut % 16 == 0
+        and rows == 8
+    )
+
+
+def pick(n, *args):
+    tokens, query_weight, memory_state = args[0], args[2], args[10]
+    experts, hidden_all = args[18].shape[0] * n, args[21].shape[1]
+    if fits(
+        n, tokens.shape[1], memory_state.shape[3], query_weight.shape[1], hidden_all, experts,
+        tokens.shape[0],
+    ):
+        return fused_shards(n, *args)
+    return shards(*args)
+
+
 def solution(mesh):
     placed = (
         P(("grp", "ep"), None),
@@ -197,7 +647,7 @@
         P(None, "ep"),
     )
     return jax.shard_map(
-        shards,
+        functools.partial(pick, mesh.shape["ep"]),
         mesh=mesh,
         in_specs=placed,
         out_specs=(

time: 196 us -> 80 us (0.41)
  waiting for transfers between devices: 112 us -> 0 us
  Pallas kernels: 0 us -> 57.5 us
  blocking collectives: 25.4 us -> 0 us
  matrix products: 17.4 us -> 0 us
  local copies, waits for them, and re-layouts: 6.97 us -> 21.3 us
  between operations: 14.2 us -> 0.65 us
  starting transfers between devices: 11.5 us -> 0 us
  other arithmetic: 7.7 us -> 0 us
    all_gather x4 -> x0, waiting for transfers between devices: 83.6 us -> none  [the longest x1 39.5 us: shards(): lax.all_gather(shared_up, 'ep', axis=0, tiled=True)]
    pallas_call x0 -> x1, Pallas kernels: none -> 57.5 us  [fused_shards(): pl.pallas_call(functools.partial(fused, n), out_shape=(jax.ShapeDtypeStru...]
    all_to_all x3 -> x0, waiting for transfers between devices: 25.4 us -> none  [the longest x1 15.8 us: shards(): lax.all_to_all(outgoing, 'ep', split_axis=0, concat_axis=0, tiled=True)]
    all_gather x1 -> x0, blocking collectives: 25.4 us -> none  [shards(): block_rows = lax.all_gather(normed, 'ep', axis=0, tiled=True)]
    dot_general x13 -> x0, matrix products: 17.4 us -> none  [the longest x4 5.03 us: shards(): jnp.dot(block_rows, matrix, preferred_element_type=jnp.float32)]
    unnamed x33 -> x14, local copies, waits for them, and re-layouts: 3.07 us -> 18.7 us
    all_to_all x3 -> x0, starting transfers between devices: 11.3 us -> none  [the longest x1 4.24 us: shards(): lax.all_to_all(result.reshape(sources, slots, width), 'ep', split_axis=0,...]
    add x1 -> x0, other arithmetic: 3.72 us -> none  [cell_step(): decay_rate[:, :, None, None] * memory_state]
  transfers between devices with their start and end apart: 7 -> 0, of which waited for: 7 -> 0; matrix products, arithmetic and copies ran while one was open for 14% -> 0% of each run, Pallas kernels for 0% -> 0%
where the time goes in v1:
time: 80 us; the launch traced here: 79.4 us
  Pallas kernels  57.5 us (72%)
  local copies, waits for them, and re-layouts  21.3 us (27%)
    pallas_call x1, Pallas kernels, fused_shards(): pl.pallas_call(functools.partial(fused, n), out_shape=(jax.ShapeDtypeStru...  57.5 us
    unnamed x14, local copies, waits for them, and re-layouts  18.7 us

profile of v1, /device:TPU:0, one launch (start us, length us, event | category | flops | bytes accessed | tf_op | source)
XLA Modules:
  0.0 79.4 jit_solution(5581174592912777951)
XLA Ops:
  0.6 1.3 %reshape.26.first_gain = bf16[1,2048]{1,0:T(2,128)(2,1)} reshape(bf16[2048]{0:T(1024)(128)(2,1)} %param.25) | data formatting | bytes 8192 | tf_op jit(solution)/shard_map/reshape | solution.py:539
  1.9 1.3 %reshape.30.second_gain = bf16[1,2048]{1,0:T(2,128)(2,1)} reshape(bf16[2048]{0:T(1024)(128)(2,1)} %param.39) | data formatting | bytes 8192 | tf_op jit(solution)/shard_map/reshape | solution.py:542
  3.2 2.0 %copy.28.query_weight = bf16[2048,64]{1,0:T(8,128)(2,1)} copy(bf16[2048,64]{0,1:T(8,128)(2,1)} %param.26) | data formatting | bytes 524288 | tf_op args[2]
  5.2 1.9 %copy.29.key_weight = bf16[2048,64]{1,0:T(8,128)(2,1)} copy(bf16[2048,64]{0,1:T(8,128)(2,1)} %param.27) | data formatting | bytes 524288 | tf_op args[3]
  7.1 2.0 %copy.30.value_weight = bf16[2048,64]{1,0:T(8,128)(2,1)} copy(bf16[2048,64]{0,1:T(8,128)(2,1)} %param.28) | data formatting | bytes 524288 | tf_op args[4]
  9.1 2.0 %copy.31.outgate_weight = bf16[2048,64]{1,0:T(8,128)(2,1)} copy(bf16[2048,64]{0,1:T(8,128)(2,1)} %param.29) | data formatting | bytes 524288 | tf_op args[5]
  11.1 1.8 %copy.32.igate_weight = bf16[2048,8]{1,0:T(8,128)(2,1)} copy(bf16[2048,8]{0,1:T(8,128)(2,1)} %param.30) | data formatting | bytes 65536 | tf_op args[6]
  12.8 1.8 %copy.33.fgate_weight = bf16[2048,8]{1,0:T(8,128)(2,1)} copy(bf16[2048,8]{0,1:T(8,128)(2,1)} %param.31) | data formatting | bytes 65536 | tf_op args[7]
  14.6 57.5 %shard_map.255 = (bf16[8,2048]{1,0:T(8,128)(2,1)}, f32[8,8,128,128]{3,2,1,0:T(8,128)}, f32[8,8,128]{2,1,0:T(8,128)}, f32[8,8]{1,0:T(8,128)}) custom-call(bf16[8,2048]{1,0:T(8,128)(2,1)} %tokens.1, bf16[1,2048]{1,0:T(2,128)(2,1)} %reshape.26.first_gain, bf16[2048,64]{1,0:T(8,128)(2,1)} %copy.28.query_weight, bf16[2048,64]{1,0:T(8,128)(2,1)} %copy.29.key_weight, ...), custom_call_target="tpu_custom_call" | custom-call | tf_op jit(solution)/shard_map/pallas_call | solution.py:547
  72.1 1.4 %copy.38 = bf16[8,2048]{1,0:T(8,128)(2,1)} copy(bf16[8,2048]{1,0:T(8,128)(2,1)} %get-tuple-element.8) | data formatting | bytes 65536
  73.5 0.0 copy-start
  73.5 0.0 copy-start.1
  73.5 4.7 %copy.39 = f32[8,8,128,128]{3,2,1,0:T(8,128)} copy(f32[8,8,128,128]{3,2,1,0:T(8,128)} %get-tuple-element.9) | data formatting | bytes 8388608
  78.2 0.0 copy-done
  78.2 0.6 copy.40
  78.8 0.0 copy-done.1
  78.8 0.6 copy.41
Async XLA Ops:
  73.5 4.7 %copy-start = (f32[8,8,128]{2,1,0:T(8,128)S(1)}, f32[8,8,128]{2,1,0:T(8,128)}, u32[]{:S(2)}) copy-start(f32[8,8,128]{2,1,0:T(8,128)} %get-tuple-element.10) | copy-start | bytes 98308
  73.5 5.3 %copy-start.1 = (f32[8,8]{1,0:T(8,128)S(1)}, f32[8,8]{1,0:T(8,128)}, u32[]{:S(2)}) copy-start(f32[8,8]{1,0:T(8,128)} %get-tuple-element.11) | copy-start | bytes 772

commit v2 on v1

--- a/solution.py
+++ b/solution.py
@@ -187,6 +187,15 @@
     )
 
 
+def across(left, right):
+    return lax.dot_general(left, right, (((1,), (1,)), ((), ())), preferred_element_type=F32)
+
+
+def in_line(gain):
+    held = gain[...].astype(F32)
+    return jnp.concatenate([held[i : i + 1] for i in range(held.shape[0])], axis=1)
+
+
 def fused(
     n,
     tokens,
@@ -217,7 +226,6 @@
     memory_next,
     norm_next,
     max_next,
-    proj_in,
     proj,
     gates_in,
     memory,
@@ -250,7 +258,7 @@
 ):
     rows, width = tokens.shape
     heads, size = memory_state.shape[1], memory_state.shape[3]
-    cut = query_weight.shape[1]
+    cut = query_weight.shape[0]
     share = size // cut
     hidden = shared_gate.shape[1] // n
     top_count = expert_ids.shape[1]
@@ -277,7 +285,7 @@
         return copy
 
     proj_loads = [
-        load(matrix, proj_in.at[i])
+        load(matrix, proj.at[pl.ds(i * cut, cut)])
         for i, matrix in enumerate((query_weight, key_weight, value_weight, outgate_weight))
     ]
     gate_loads = [load(igate_weight, gates_in.at[0]), load(fgate_weight, gates_in.at[1])]
@@ -294,7 +302,7 @@
     down_load = load(expert_down.at[0], down)
 
     inputs = tokens[...].astype(F32)
-    rows_one[me] = rms_scale(inputs, first_gain[...]).astype(BF16)
+    rows_one[me] = rms_scale(inputs, in_line(first_gain)).astype(BF16)
 
     pl.semaphore_wait(barrier, n - 1)
 
@@ -343,10 +351,6 @@
     unsent = []
     first = gather(rows_one, 0)
 
-    for copy in proj_loads:
-        copy.wait()
-    for i in range(4):
-        proj[:, i * cut : (i + 1) * cut] = proj_in[i]
     for i in range(1, share):
         other = pl.multiple_of(((me + i) % share) * cut, cut)
         out_pad[pl.ds(other, cut), :] = jnp.zeros((cut, width), BF16)
@@ -363,10 +367,8 @@
     for copy in gate_loads:
         copy.wait()
     own = rows_one[me]
-    input_gate = jnp.dot(own, gates_in[0], preferred_element_type=F32) + igate_bias[...]
-    forget_log = jax.nn.log_sigmoid(
-        jnp.dot(own, gates_in[1], preferred_element_type=F32) + fgate_bias[...]
-    )
+    input_gate = across(own, gates_in[0]) + igate_bias[...]
+    forget_log = jax.nn.log_sigmoid(across(own, gates_in[1]) + fgate_bias[...])
     kept = forget_log + max_state[...]
     top = jnp.maximum(kept, input_gate)
     max_next[...] = top
@@ -380,7 +382,9 @@
         held = buffer[...].astype(F32)
         return held.reshape(n * rows, held.shape[2])
 
-    columns = jnp.dot(flat(rows_one).astype(BF16), proj[...], preferred_element_type=F32)
+    for copy in proj_loads:
+        copy.wait()
+    columns = across(flat(rows_one).astype(BF16), proj[...])
     column_send[...] = columns.reshape(n, rows, 4 * cut).astype(BF16)
 
     def spread(which, source, target):
@@ -487,7 +491,7 @@
         0, None, jnp.dot(flat(gated_recv).astype(BF16), out_pad[...], preferred_element_type=F32)
     )
     stream = tokens[...].astype(F32) + mix.astype(BF16).astype(F32)
-    rows_two[me] = rms_scale(stream, second_gain[...]).astype(BF16)
+    rows_two[me] = rms_scale(stream, in_line(second_gain)).astype(BF16)
     second = gather(rows_two, 1)
     for copy in wide_loads + [down_load]:
         copy.wait()
@@ -505,9 +509,7 @@
     gate_sums = jnp.dot(block, wide[0], preferred_element_type=F32)
     up_sums = jnp.dot(block, wide[1], preferred_element_type=F32)
     own_hidden = (jax.nn.silu(gate_sums) * up_sums).astype(BF16)
-    both = lax.dot_general(
-        block, shared_wide, (((1,), (1,)), ((), ())), preferred_element_type=F32
-    )
+    both = across(block, shared_wide)
     shared_hidden = (jax.nn.silu(both[:, :hidden]) * both[:, hidden:]).astype(BF16)
     value = weight * jnp.dot(own_hidden, down[...], preferred_element_type=F32) + jnp.dot(
         shared_hidden, shared_rows, preferred_element_type=F32
@@ -536,10 +538,10 @@
     chips = n // 2
     inner = expert_gate.shape[2]
     operands = (
-        tokens, first_gain.reshape(1, -1), query_weight, key_weight, value_weight, outgate_weight,
-        igate_weight, fgate_weight, igate_bias.reshape(1, -1), fgate_bias.reshape(1, -1),
+        tokens, first_gain.reshape(-1, 128), query_weight.T, key_weight.T, value_weight.T,
+        outgate_weight.T, igate_weight.T, fgate_weight.T, igate_bias.reshape(1, -1), fgate_bias.reshape(1, -1),
         memory_state, norm_state, max_state, head_gain.reshape(heads, size), out_weight,
-        second_gain.reshape(1, -1), expert_ids, route_weight, expert_gate, expert_up, expert_down,
+        second_gain.reshape(-1, 128), expert_ids, route_weight, expert_gate, expert_up, expert_down,
         shared_gate, shared_up, shared_down.reshape(n, hidden, shared_down.shape[1]),
     )
     far = {2, 3, 4, 5, 6, 7, 10, 14, 18, 19, 20}
@@ -557,9 +559,8 @@
         ],
         out_specs=tuple(pl.BlockSpec(memory_space=m) for m in (VMEM, ANY, VMEM, VMEM)),
         scratch_shapes=[
-            VMEM((4, width, cut), BF16),
-            VMEM((width, 4 * cut), BF16),
-            VMEM((2, width, heads), BF16),
+            VMEM((4 * cut, width), BF16),
+            VMEM((2, heads, width), BF16),
             VMEM(memory_state.shape, F32),
             VMEM((size, width), BF16),
             VMEM((2, width, inner), BF16),

time: 80 us -> 66 us (0.82)
  local copies, waits for them, and re-layouts: 21.3 us -> 7.29 us
    unnamed x14 -> x8, local copies, waits for them, and re-layouts: 18.7 us -> 7.29 us
    reshape x2 -> x0, local copies, waits for them, and re-layouts: 2.58 us -> none  [the longest x1 1.29 us: fused_shards(): first_gain.reshape(1, -1)]
where the time goes in v2:
time: 66 us; the launch traced here: 65.8 us
  Pallas kernels  57.9 us (88%)
  local copies, waits for them, and re-layouts  7.29 us (11%)
    pallas_call x1, Pallas kernels, fused_shards(): pl.pallas_call(functools.partial(fused, n), out_shape=(jax.ShapeDtypeStru...  57.9 us
    unnamed x8, local copies, waits for them, and re-layouts  7.29 us

profile of v2, /device:TPU:0, one launch (start us, length us, event | category | flops | bytes accessed | tf_op | source)
XLA Modules:
  0.0 65.8 jit_solution(16653285308880784674)
XLA Ops:
  0.6 57.9 %shard_map.255 = (bf16[8,2048]{1,0:T(8,128)(2,1)}, f32[8,8,128,128]{3,2,1,0:T(8,128)}, f32[8,8,128]{2,1,0:T(8,128)}, f32[8,8]{1,0:T(8,128)}) custom-call(bf16[8,2048]{1,0:T(8,128)(2,1)} %tokens.1, bf16[16,128]{1,0:T(8,128)(2,1)} %bitcast.19, bf16[64,2048]{1,0:T(8,128)(2,1)} %bitcast.12, bf16[64,2048]{1,0:T(8,128)(2,1)} %bitcast.13, ...), custom_call_target="tpu_custom_call" | custom-call | tf_op jit(solution)/shard_map/pallas_call | solution.py:549
  58.5 1.4 %copy.32 = bf16[8,2048]{1,0:T(8,128)(2,1)} copy(bf16[8,2048]{1,0:T(8,128)(2,1)} %get-tuple-element.8) | data formatting | bytes 65536
  59.9 0.0 copy-start
  59.9 0.0 copy-start.1
  59.9 4.7 %copy.33 = f32[8,8,128,128]{3,2,1,0:T(8,128)} copy(f32[8,8,128,128]{3,2,1,0:T(8,128)} %get-tuple-element.9) | data formatting | bytes 8388608
  64.6 0.0 copy-done
  64.6 0.6 copy.34
  65.2 0.0 copy-done.1
  65.2 0.6 copy.35
Async XLA Ops:
  59.9 4.7 %copy-start = (f32[8,8,128]{2,1,0:T(8,128)S(1)}, f32[8,8,128]{2,1,0:T(8,128)}, u32[]{:S(2)}) copy-start(f32[8,8,128]{2,1,0:T(8,128)} %get-tuple-element.10) | copy-start | bytes 98308
  59.9 5.3 %copy-start.1 = (f32[8,8]{1,0:T(8,128)S(1)}, f32[8,8]{1,0:T(8,128)}, u32[]{:S(2)}) copy-start(f32[8,8]{1,0:T(8,128)} %get-tuple-element.11) | copy-start | bytes 772

commit v3 on v2

--- a/solution.py
+++ b/solution.py
@@ -249,7 +249,6 @@
     sum_recv,
     local_sem,
     memory_in_sem,
-    memory_out_sem,
     send_sem,
     recv_sem,
     gather_sem,
@@ -411,7 +410,6 @@
     spread(3, lambda j: shared_down.at[j], sdown_recv.at[me])
     sdown_recv[me] = shared_down[me]
 
-    memory_stores = []
     for h in range(heads):
         pieces = [column_recv[h * share + i].astype(F32) for i in range(share)]
         query, keyed, valued, outgate = [
@@ -433,13 +431,8 @@
                 decay[s : s + 1, :] * memory[s, h]
                 + key_columns[:, s : s + 1] * valued[s : s + 1, :]
             )
-            memory[s, h] = cell
+            memory_next[s, h] = cell
             tops.append(jnp.sum(query_columns[:, s : s + 1] * cell, axis=0, keepdims=True))
-        store = pltpu.make_async_copy(
-            memory.at[:, h], memory_next.at[:, h], memory_out_sem.at[h]
-        )
-        store.start()
-        memory_stores.append(store)
         readout = jnp.concatenate(tops, axis=0) / bottom
         readout = rms_scale(readout, head_gain[h : h + 1, :])
         gated_send[h] = (readout * jax.nn.sigmoid(outgate)).astype(BF16)
@@ -518,8 +511,6 @@
 
     for copy in unsent:
         copy.wait_send()
-    for copy in memory_stores:
-        copy.wait()
 
 
 def ORDER(chips):
@@ -545,6 +536,10 @@
         shared_gate, shared_up, shared_down.reshape(n, hidden, shared_down.shape[1]),
     )
     far = {2, 3, 4, 5, 6, 7, 10, 14, 18, 19, 20}
+    operands = [
+        pltpu.with_memory_space_constraint(x, pltpu.HBM)
+        for i, x in enumerate(operands)
+    ]
     dma = pltpu.SemaphoreType.DMA
     return pl.pallas_call(
         functools.partial(fused, n),
@@ -555,9 +550,9 @@
             jax.ShapeDtypeStruct(max_state.shape, F32),
         ),
         in_specs=[
-            pl.BlockSpec(memory_space=ANY if i in far else VMEM) for i in range(len(operands))
+            pl.BlockSpec(memory_space=pltpu.HBM if i in far else VMEM) for i in range(len(operands))
         ],
-        out_specs=tuple(pl.BlockSpec(memory_space=m) for m in (VMEM, ANY, VMEM, VMEM)),
+        out_specs=tuple(pl.BlockSpec(memory_space=m) for m in (VMEM, VMEM, VMEM, VMEM)),
         scratch_shapes=[
             VMEM((4 * cut, width), BF16),
             VMEM((2, heads, width), BF16),
@@ -582,7 +577,6 @@
             VMEM((2, chips, rows, width), BF16),
             dma((10,)),
             dma((heads,)),
-            dma((heads,)),
             dma((5, n)),
             dma((5, n)),
             dma((2, 4, chips)),
@@ -590,7 +584,7 @@
             dma((2, 2, chips)),
         ],
         compiler_params=pltpu.CompilerParams(
-            collective_id=0, has_side_effects=True, vmem_limit_bytes=60 * 1024 * 1024
+            collective_id=0, has_side_effects=True, vmem_limit_bytes=28 * 1024 * 1024
         ),
     )(*operands)
 

time: 66 us -> 61.8 us (0.936)
  local copies, waits for them, and re-layouts: 7.29 us -> 3.84 us
  Pallas kernels: 57.9 us -> 57.2 us
    unnamed x8 -> x4, local copies, waits for them, and re-layouts: 7.29 us -> 3.84 us
    pallas_call x1, Pallas kernels: 57.9 us -> 57.2 us  [fused_shards(): pl.pallas_call(functools.partial(fused, n), out_shape=(jax.ShapeDtypeStru...]
where the time goes in v3:
time: 61.8 us; the launch traced here: 61.6 us
  Pallas kernels  57.2 us (93%)
  local copies, waits for them, and re-layouts  3.84 us (6%)
  between operations  0.65 us (1%)
    pallas_call x1, Pallas kernels, fused_shards(): pl.pallas_call(functools.partial(fused, n), out_shape=(jax.ShapeDtypeStru...  57.2 us
    unnamed x4, local copies, waits for them, and re-layouts  3.84 us

profile of v3, /device:TPU:0, one launch (start us, length us, event | category | flops | bytes accessed | tf_op | source)
XLA Modules:
  0.0 61.6 jit_solution(16236311474885947285)
XLA Ops:
  0.6 57.2 %shard_map.255 = (bf16[8,2048]{1,0:T(8,128)(2,1)S(1)}, f32[8,8,128,128]{3,2,1,0:T(8,128)S(1)}, f32[8,8,128]{2,1,0:T(8,128)S(1)}, f32[8,8]{1,0:T(8,128)S(1)}) custom-call(bf16[8,2048]{1,0:T(8,128)(2,1)} %tokens.1, bf16[16,128]{1,0:T(8,128)(2,1)} %bitcast.19, bf16[64,2048]{1,0:T(8,128)(2,1)} %bitcast.12, bf16[64,2048]{1,0:T(8,128)(2,1)} %bitcast.13, ...), custom_call_target="tpu_custom_call" | custom-call | tf_op jit(solution)/shard_map/pallas_call | solution.py:544
  57.8 0.6 %copy.32 = bf16[8,2048]{1,0:T(8,128)(2,1)} copy(bf16[8,2048]{1,0:T(8,128)(2,1)S(1)} %get-tuple-element.8) | data formatting | bytes 65536
  58.4 2.0 %copy.33 = f32[8,8,128,128]{3,2,1,0:T(8,128)} copy(f32[8,8,128,128]{3,2,1,0:T(8,128)S(1)} %get-tuple-element.9) | data formatting | bytes 8388608
  60.4 0.6 copy.34
  61.0 0.6 copy.35
